TPU v7x, 32 devices: a whole 2x2x4 slice. The times are simulated.
32 devices in a mesh: kv: 8 (over z, x), tp: 4 (over y, core).
Axes of the slice: x: 2, y: 2, z: 4, core: 2. Of those that a mesh axis runs over, the one named last changes fastest.
Arguments:
- queries: bfloat16 [1024, 2048], P('kv', 'tp'), may hold values from -6 to 6
- keys: bfloat16 [1024, 2048], P('kv', 'tp'), may hold values from -6 to 6
- values: bfloat16 [1024, 2048], P('kv', 'tp'), may hold values from -6 to 6
- attended: bfloat16 [1024, 2048], P('kv', 'tp'), may hold values from -6 to 6
- cotangent: bfloat16 [1024, 2048], P('kv', 'tp'), may hold values from -96 to 96
- log_totals: float32 [32, 1024], P('tp', 'kv'), may hold values from 4 to 7
- block_picks: int32 [32, 16, 8], P('tp', 'kv'), may hold values from -1 to 14, as said below
- normed: bfloat16 [1024, 4096], P('kv', 'tp'), may hold values from -6 to 6
Outputs:
- grad_queries: bfloat16 [1024, 2048], P('kv', 'tp')
- grad_keys: bfloat16 [1024, 2048], P('kv', 'tp')
- grad_values: bfloat16 [1024, 2048], P('kv', 'tp')
- grad_weight: float32 [4096, 2048], P('kv', 'tp')
Inputs may be any that keep to these rules, and one draw needn't show every extreme that they name: `block_picks`: row c of head h names at most 8 distinct blocks below c, followed by -1 in the other slots. One key block is named by at most 4 query blocks of one head, and in every draw each head has a block named exactly 4 times.
All inputs are finite; a program needn't handle non-finite values.
Results may differ from a plain program's by a relative error of at most 0.0069.
Values may be sent and summed in bfloat16 or wider, within the bound.
A program may use at most 128 MiB of HBM per device.

v0:
```python
import functools

import jax
import jax.numpy as jnp
from jax import lax
from jax.experimental import pallas as pl
from jax.experimental.pallas import tpu as pltpu
from jax.sharding import PartitionSpec as P

BLOCK = 64


def tile_terms(q_tile, k_tile, v_tile, g_tile, log_total, row_dots, allowed):
    scale = q_tile.shape[-1] ** (-0.5)
    scores = (
        jnp.einsum("...qd,...kd->...qk", q_tile, k_tile, preferred_element_type=jnp.float32) * scale
    )
    probs = jnp.where(allowed, jnp.exp(scores - log_total[..., None]), 0.0)
    probs_low = probs.astype(jnp.bfloat16)
    grad_v = jnp.einsum("...qk,...qd->...kd", probs_low, g_tile, preferred_element_type=jnp.float32)
    grad_p = jnp.einsum("...qd,...kd->...qk", g_tile, v_tile, preferred_element_type=jnp.float32)
    grad_s = (probs * (grad_p - row_dots[..., None])).astype(jnp.bfloat16)
    grad_q = (
        jnp.einsum("...qk,...kd->...qd", grad_s, k_tile, preferred_element_type=jnp.float32) * scale
    )
    grad_k = (
        jnp.einsum("...qk,...qd->...kd", grad_s, q_tile, preferred_element_type=jnp.float32) * scale
    )
    return (grad_q, grad_k, grad_v)


def add_by_block(tiles, segments, block_total):
    onehot = (segments[..., None] == jnp.arange(block_total)).astype(jnp.float32)
    return jnp.einsum("hnb,hnkd->hbkd", onehot, tiles, precision=lax.Precision.HIGHEST)


def local(queries, keys, values, attended, cotangent, log_totals, block_picks, normed):
    tok_rows, row_width = queries.shape
    head_count = log_totals.shape[0]
    head_size = row_width // head_count
    local_blocks = tok_rows // BLOCK
    kv_count = lax.axis_size("kv")
    all_blocks = local_blocks * kv_count

    def by_head(matrix, blocks):
        return matrix.reshape(blocks, BLOCK, head_count, head_size).transpose(2, 0, 1, 3)

    def to_rows(tensor):
        return tensor.transpose(1, 2, 0, 3).reshape(tensor.shape[1] * BLOCK, row_width)

    q_heads = by_head(queries, local_blocks)
    k_heads = by_head(keys, local_blocks)
    v_heads = by_head(values, local_blocks)
    g_heads = by_head(cotangent, local_blocks)
    o_heads = by_head(attended, local_blocks)
    log_heads = log_totals.reshape(head_count, local_blocks, BLOCK)
    row_dots = jnp.einsum("hbqd,hbqd->hbq", g_heads, o_heads, preferred_element_type=jnp.float32)
    causal = jnp.tril(jnp.ones((BLOCK, BLOCK), bool))
    dq_diag, dk_diag, dv_diag = tile_terms(
        q_heads, k_heads, v_heads, g_heads, log_heads, row_dots, causal
    )
    q_all, g_all = (
        lax.all_gather(queries, "kv", axis=0, tiled=True),
        lax.all_gather(cotangent, "kv", axis=0, tiled=True),
    )
    log_all, dots_all = (
        lax.all_gather(log_totals, "kv", axis=1, tiled=True),
        lax.all_gather(row_dots.reshape(head_count, tok_rows), "kv", axis=1, tiled=True),
    )
    picks_all = lax.all_gather(block_picks, "kv", axis=1, tiled=True)
    most = max(2, all_blocks // 4)
    own_ids = lax.axis_index("kv") * local_blocks + jnp.arange(local_blocks)
    matched = jnp.any(picks_all[:, :, :, None] == own_ids, axis=2)
    position = jnp.cumsum(matched.astype(jnp.int32), axis=1) - 1
    slot_hit = matched[..., None] & (position[..., None] == jnp.arange(most))
    listed = jnp.sum(jnp.where(slot_hit, jnp.arange(all_blocks)[None, :, None, None], 0), axis=1)
    filled = jnp.any(slot_hit, axis=1)
    q_blocks = by_head(q_all, all_blocks)
    g_blocks = by_head(g_all, all_blocks)
    log_blocks = log_all.reshape(head_count, all_blocks, BLOCK)
    dots_blocks = dots_all.reshape(head_count, all_blocks, BLOCK)
    q_sel = jax.vmap(lambda t, i: t[i])(q_blocks, listed)
    g_sel = jax.vmap(lambda t, i: t[i])(g_blocks, listed)
    l_sel = jax.vmap(lambda t, i: t[i])(log_blocks, listed)
    d_sel = jax.vmap(lambda t, i: t[i])(dots_blocks, listed)
    tile_shape = q_sel.shape
    k_rep = jnp.broadcast_to(k_heads[:, :, None], tile_shape)
    v_rep = jnp.broadcast_to(v_heads[:, :, None], tile_shape)
    allowed = jnp.broadcast_to(filled[..., None, None], tile_shape[:4] + (BLOCK,))
    dq_sel, dk_sel, dv_sel = tile_terms(q_sel, k_rep, v_rep, g_sel, l_sel, d_sel, allowed)
    grad_k = to_rows(dk_diag + jnp.sum(dk_sel, axis=2))
    grad_v = to_rows(dv_diag + jnp.sum(dv_sel, axis=2))
    segments = jnp.where(filled, listed, all_blocks).reshape(head_count, local_blocks * most)
    dq_blocks = add_by_block(
        dq_sel.reshape(head_count, local_blocks * most, BLOCK, head_size), segments, all_blocks
    )
    dq_full = to_rows(dq_blocks)
    remote_q = lax.psum_scatter(dq_full, "kv", scatter_dimension=0, tiled=True)
    grad_queries = (remote_q + to_rows(dq_diag)).astype(jnp.bfloat16)
    full_hidden = lax.all_gather(normed, "tp", axis=1, tiled=True)
    grad_weight = lax.psum_scatter(
        lax.dot_general(
            full_hidden, grad_queries, (((0,), (0,)), ((), ())), preferred_element_type=jnp.float32
        ),
        "kv",
        scatter_dimension=0,
        tiled=True,
    )
    return (grad_queries, grad_k.astype(jnp.bfloat16), grad_v.astype(jnp.bfloat16), grad_weight)


def head_grads(q, k, v, g, log_total, row_dots, picks):
    rows = q.shape[0]
    blocks = rows // BLOCK
    scale = q.shape[-1] ** (-0.5)
    contract_last = (((1,), (1,)), ((), ()))
    contract_first = (((0,), (0,)), ((), ()))
    chosen = jnp.any(picks[:, :, None] == jnp.arange(blocks), axis=1)
    position = jnp.arange(rows)
    chosen = jnp.repeat(jnp.repeat(chosen, BLOCK, axis=0), BLOCK, axis=1)
    own = (position[:, None] // BLOCK == position[None, :] // BLOCK) & (
        position[:, None] >= position[None, :]
    )
    scores = lax.dot_general(q, k, contract_last, preferred_element_type=jnp.float32) * scale
    probs = jnp.where(chosen | own, jnp.exp(scores - log_total[:, None]), 0.0)
    grad_p = lax.dot_general(g, v, contract_last, preferred_element_type=jnp.float32)
    grad_s = (probs * (grad_p - row_dots[:, None])).astype(jnp.bfloat16)
    grad_v = lax.dot_general(
        probs.astype(jnp.bfloat16), g, contract_first, preferred_element_type=jnp.float32
    )
    grad_k = lax.dot_general(grad_s, q, contract_first, preferred_element_type=jnp.float32) * scale
    grad_q = jnp.dot(grad_s, k, preferred_element_type=jnp.float32) * scale
    return grad_q.astype(jnp.bfloat16), grad_k.astype(jnp.bfloat16), grad_v.astype(jnp.bfloat16)


def by_heads(queries, keys, values, attended, cotangent, log_totals, block_picks, normed):
    tok_rows, row_width = queries.shape
    head_count = log_totals.shape[0]
    head_size = row_width // head_count
    kv_count = lax.axis_size("kv")
    heads = head_count // kv_count
    product = cotangent.astype(jnp.float32) * attended.astype(jnp.float32)
    row_dots = jnp.sum(product.reshape(tok_rows, head_count, head_size), axis=2).T
    packed = lax.all_to_all(
        jnp.stack([queries, keys, values, cotangent]), "kv", split_axis=2, concat_axis=1, tiled=True
    )
    sides = lax.all_to_all(
        jnp.stack([log_totals, row_dots]), "kv", split_axis=1, concat_axis=2, tiled=True
    )
    picks = lax.all_to_all(block_picks, "kv", split_axis=0, concat_axis=1, tiled=True)
    features = lax.all_gather(normed, "tp", axis=1, tiled=True)
    features = lax.all_to_all(features, "kv", split_axis=1, concat_axis=0, tiled=True)
    grads = []
    for h in range(heads):
        q, k, v, g = (packed[i, :, h * head_size : (h + 1) * head_size] for i in range(4))
        grads.append(head_grads(q, k, v, g, sides[0, h], sides[1, h], picks[h]))
    dq, dk, dv = (jnp.concatenate(parts, axis=1) for parts in zip(*grads))
    dq_all = lax.all_gather(dq, "kv", axis=1, tiled=True)
    dkv = lax.all_to_all(jnp.stack([dk, dv]), "kv", split_axis=1, concat_axis=2, tiled=True)
    grad_queries = lax.dynamic_slice_in_dim(
        dq_all, lax.axis_index("kv") * tok_rows, tok_rows, axis=0
    )
    grad_weight = lax.dot_general(
        features, dq_all, (((0,), (0,)), ((), ())), preferred_element_type=jnp.float32
    )
    return (grad_queries, dkv[0], dkv[1], grad_weight)


NEVER = -1e30
LAST = (((1,), (1,)), ((), ()))
FIRST = (((0,), (0,)), ((), ()))


def mm(a, b, dims=(((1,), (0,)), ((), ()))):
    return lax.dot_general(a, b, dims, preferred_element_type=jnp.float32)


def remote(src, dst, send, recv, kv, tp):
    return pltpu.make_async_remote_copy(
        src_ref=src,
        dst_ref=dst,
        send_sem=send,
        recv_sem=recv,
        device_id=(kv, tp),
        device_id_type=pl.DeviceIdType.MESH,
    )


def one_head_kernel(
    kvs, tps, q_hbm, k_hbm, v_hbm, g_hbm, o_hbm, log_hbm, picks_hbm, n_hbm,
    gq_ref, gk_ref, gv_ref, gw_ref,
    q_ref, k_ref, v_ref, g_ref, o_ref, log_ref, picks_ref, n_ref, load,
    sent, sent_side, got, got_side, turned, feats, total, dq_all, dkv, dkv_got,
    in_send, in_recv, side_send, side_recv, n1_send, n1_recv, n2_send, n2_recv,
    up_send, down_send, mate_send, line_recv, mate_recv, dkv_send, dkv_recv,
):
    me, tp = lax.axis_index("kv"), lax.axis_index("tp")
    rows, width = q_ref.shape
    hs = width // kvs
    per = rows // BLOCK
    scale = hs ** (-0.5)
    ratio = kvs // tps
    part = feats.shape[1]

    loads = []
    pairs = ((q_hbm, q_ref), (k_hbm, k_ref), (v_hbm, v_ref), (g_hbm, g_ref), (o_hbm, o_ref))
    pairs += ((log_hbm, log_ref), (picks_hbm, picks_ref), (n_hbm, n_ref))
    for at, (source, place) in enumerate(pairs):
        loads.append(pltpu.make_async_copy(source, place, load.at[at]))
        loads[-1].start()

    barrier = pltpu.get_barrier_semaphore()
    count = kvs * tps

    def greet(step, carry):
        other = lax.rem(me * tps + tp + step, count)
        pl.semaphore_signal(
            barrier,
            inc=1,
            device_id=(other // tps, lax.rem(other, tps)),
            device_id_type=pl.DeviceIdType.MESH,
        )
        return carry

    lax.fori_loop(1, count, greet, 0)
    for copy in loads[:-1]:
        copy.wait()

    for h in range(kvs):
        c = slice(h * hs, (h + 1) * hs)
        sent[h, :, : 2 * hs] = jnp.concatenate([q_ref[:, c], k_ref[:, c]], axis=1)
        sent[h, :, 2 * hs :] = jnp.concatenate([v_ref[:, c], g_ref[:, c]], axis=1)
    product = g_ref[...].astype(jnp.float32) * o_ref[...].astype(jnp.float32)
    high = product.astype(jnp.bfloat16)
    low = (product - high.astype(jnp.float32)).astype(jnp.bfloat16)
    head_of = lax.broadcasted_iota(jnp.int32, (16, width), 1) // hs
    pick = (head_of == lax.broadcasted_iota(jnp.int32, (16, width), 0)).astype(jnp.bfloat16)
    dots = mm(pick, high, LAST) + mm(pick, low, LAST)
    line = lax.broadcasted_iota(jnp.int32, (8, rows), 0)
    block_at = lax.broadcasted_iota(jnp.int32, (8, rows), 1) // BLOCK
    for h in range(kvs):
        lines = jnp.where(line == 1, dots[h : h + 1], -log_ref[h : h + 1])
        for b in range(per):
            named = picks_ref[h, b : b + 1]
            bit = jnp.where(named >= 0, jnp.left_shift(1, jnp.maximum(named, 0)), 0)
            bits = jnp.sum(bit.astype(jnp.float32), axis=1, keepdims=True)
            here_in = jnp.logical_and(line == 2, block_at == b)
            lines = jnp.where(here_in, bits, lines)
        sent_side[h] = lines
    got[me] = sent[me]
    got_side[me] = sent_side[me]

    pl.semaphore_wait(barrier, count - 1)

    waits = []
    for d in range(1, kvs):
        to = lax.rem(me + d, kvs)
        side = remote(
            sent_side.at[to], got_side.at[me], side_send.at[d], side_recv.at[d], to, tp
        )
        main = remote(sent.at[to], got.at[me], in_send.at[d], in_recv.at[d], to, tp)
        side.start()
        main.start()
        waits += [side, main]

    loads[-1].wait()
    for b in range(n_ref.shape[1] // 128):
        c = slice(b * 128, (b + 1) * 128)
        turned[c, :] = n_ref[:, c].astype(jnp.float32).T.astype(jnp.bfloat16)
    here = pl.ds(pl.multiple_of(me * rows, rows), rows)

    def n1_copy(h, j):
        place = (h * tps + j) * part
        return remote(
            turned.at[pl.ds(place, part)],
            feats.at[j, :, here],
            n1_send.at[h * tps + j],
            n1_recv.at[me],
            ratio * tp + h,
            j,
        )

    for h in range(ratio):
        for j in range(tps):
            mine = jnp.logical_and(me == ratio * tp + h, tp == j)

            @pl.when(jnp.logical_not(mine))
            def _():
                n1_copy(h, j).start()

            @pl.when(mine)
            def _():
                place = (h * tps + j) * part
                feats[j, :, here] = turned[place : place + part, :]

    for d in range(1, kvs):
        src = lax.rem(me + kvs - d, kvs)
        remote(
            sent_side.at[src], got_side.at[src], side_send.at[d], side_recv.at[d], src, tp
        ).wait_recv()
        remote(sent.at[src], got.at[src], in_send.at[d], in_recv.at[d], src, tp).wait_recv()

    s_at = lax.broadcasted_iota(jnp.int32, (rows, rows), 0)
    t_at = lax.broadcasted_iota(jnp.int32, (rows, rows), 1)
    own = jnp.logical_and(s_at // BLOCK == t_at // BLOCK, s_at <= t_at)
    lines = [
        jnp.concatenate([got_side[m, r : r + 1] for m in range(kvs)], axis=1) for r in range(3)
    ]
    for i in range(kvs):
        late = (kvs - i) * rows
        q = got[i:, :, :hs].reshape(late, hs)
        g = got[i:, :, 3 * hs :].reshape(late, hs)
        k = got[i, :, hs : 2 * hs]
        v = got[i, :, 2 * hs : 3 * hs]

        minus, dots, bits = (r[:, i * rows :] for r in lines)
        bits = bits.astype(jnp.int32)
        parts = []
        for b in range(per):
            named = jnp.bitwise_and(lax.shift_right_logical(bits, i * per + b), 1) == 1
            parts.append(jnp.broadcast_to(jnp.where(named, minus, NEVER), (BLOCK, late)))
        bias = jnp.concatenate(parts, axis=0)
        first = jnp.where(own, minus[:, :rows], bias[:, :rows])
        bias = first if i == kvs - 1 else jnp.concatenate([first, bias[:, rows:]], axis=1)
        probs = jnp.exp(mm(k, q, LAST) * scale + bias)
        grad_s = (probs * (mm(v, g, LAST) - dots)).astype(jnp.bfloat16)
        grad_v = mm(probs.astype(jnp.bfloat16), g)
        grad_k = mm(grad_s, q) * scale
        dkv[i] = jnp.concatenate([grad_k, grad_v], axis=1).astype(jnp.bfloat16)
        grad_q = mm(k, grad_s, FIRST)
        if i == 0:
            total[...] = grad_q
        else:
            total[:, i * rows :] += grad_q
    dq_all[me] = (total[...] * scale).astype(jnp.bfloat16)
    dkv_got[me] = dkv[me]

    deep = kvs // 2
    spot, side_of = me // 2, lax.rem(me, 2)
    mate = me + 1 - 2 * side_of
    half = hs // 2
    not_top, not_bottom = spot < deep - 1, spot > 0

    def unit_copy(unit, piece, send, recv, column, to):
        rows_of = dq_all.at[unit * 2 + column, piece * half : (piece + 1) * half]
        at = unit * 2 + piece
        return remote(rows_of, rows_of, send.at[at], recv.at[at], to, tp)

    def upward(unit, piece):
        return unit_copy(unit, piece, up_send, line_recv, side_of, me + 2)

    def downward(unit, piece):
        return unit_copy(unit, piece, down_send, line_recv, side_of, me - 2)

    def across(unit, piece):
        return unit_copy(unit, piece, mate_send, mate_recv, side_of, mate)

    for piece in range(2):

        @pl.when(not_top)
        def _():
            upward(spot, piece).start()

        @pl.when(not_bottom)
        def _():
            downward(spot, piece).start()

    for piece in range(2):
        across(spot, piece).start()
    for d in range(1, kvs):
        to = lax.rem(me + d, kvs)
        copy = remote(dkv.at[to], dkv_got.at[me], dkv_send.at[d], dkv_recv.at[d], to, tp)
        copy.start()
        waits.append(copy)

    for k in range(kvs):

        @pl.when(jnp.logical_not(jnp.logical_and(me == k, tp == me // ratio)))
        def _():
            remote(
                turned.at[pl.ds(0, part)],
                feats.at[tp, :, pl.ds(k * rows, rows)],
                n1_send.at[0],
                n1_recv.at[k],
                me,
                tp,
            ).wait_recv()

    for d in range(1, tps):
        to = lax.rem(tp + d, tps)
        copy = remote(feats.at[tp], feats.at[tp], n2_send.at[d], n2_recv.at[d], me, to)
        copy.start()
        waits.append(copy)

    for z in range(1, deep):
        for piece in range(2):

            @pl.when(spot >= z)
            def _():
                unit_copy(spot - z, piece, up_send, line_recv, side_of, me).wait_recv()

                @pl.when(not_top)
                def _():
                    upward(spot - z, piece).start()

                across(spot - z, piece).start()

            @pl.when(spot + z < deep)
            def _():
                unit_copy(spot + z, piece, down_send, line_recv, side_of, me).wait_recv()

                @pl.when(not_bottom)
                def _():
                    downward(spot + z, piece).start()

                across(spot + z, piece).start()

    for d in range(1, kvs):
        src = lax.rem(me + kvs - d, kvs)
        remote(
            dkv.at[src], dkv_got.at[src], dkv_send.at[d], dkv_recv.at[d], src, tp
        ).wait_recv()
    for p in range(kvs // 2):
        c = slice(p * 2 * hs, (p + 1) * 2 * hs)
        left, right = dkv_got[2 * p], dkv_got[2 * p + 1]
        gk_ref[:, c] = jnp.concatenate([left[:, :hs], right[:, :hs]], axis=1)
        gv_ref[:, c] = jnp.concatenate([left[:, hs:], right[:, hs:]], axis=1)

    for d in range(1, tps):
        src = lax.rem(tp + tps - d, tps)
        remote(
            feats.at[src], feats.at[src], n2_send.at[d], n2_recv.at[d], me, src
        ).wait_recv()
    step = jnp.where(spot < deep // 2, 1, deep - 1)
    for z in range(deep):
        unit = lax.rem(spot + z * step, deep)
        for piece in range(2):
            unit_copy(unit, piece, mate_send, mate_recv, 1 - side_of, me).wait_recv()
        c = pl.ds(pl.multiple_of(unit * 2 * hs, 2 * hs), 2 * hs)
        pair = dq_all[pl.ds(unit * 2, 2), :, here].reshape(2 * hs, rows)
        gq_ref[:, c] = pair.astype(jnp.float32).T.astype(jnp.bfloat16)
        cols = dq_all[pl.ds(unit * 2, 2)].reshape(2 * hs, kvs * rows)
        for j in range(tps):
            gw_ref[j * part : (j + 1) * part, c] = mm(feats[j], cols, LAST)

    for unit in range(deep):
        for piece in range(2):
            across(unit, piece).wait_send()

            @pl.when(jnp.logical_and(not_top, unit <= spot))
            def _():
                upward(unit, piece).wait_send()

            @pl.when(jnp.logical_and(not_bottom, unit >= spot))
            def _():
                downward(unit, piece).wait_send()

    for copy in waits:
        copy.wait_send()
    for h in range(ratio):
        for j in range(tps):
            mine = jnp.logical_and(me == ratio * tp + h, tp == j)

            @pl.when(jnp.logical_not(mine))
            def _():
                n1_copy(h, j).wait_send()


def one_head(queries, keys, values, attended, cotangent, log_totals, block_picks, normed):
    rows, width = queries.shape
    kvs, tps = lax.axis_size("kv"), lax.axis_size("tp")
    hs = width // kvs
    local_width = normed.shape[1]
    part = local_width // kvs
    vmem = pl.BlockSpec(memory_space=pltpu.VMEM)
    dma = pltpu.SemaphoreType.DMA
    low = jnp.bfloat16
    return pl.pallas_call(
        functools.partial(one_head_kernel, kvs, tps),
        out_shape=(
            jax.ShapeDtypeStruct((rows, width), low),
            jax.ShapeDtypeStruct((rows, width), low),
            jax.ShapeDtypeStruct((rows, width), low),
            jax.ShapeDtypeStruct((tps * part, width), jnp.float32),
        ),
        in_specs=[pl.BlockSpec(memory_space=pl.ANY)] * 8,
        out_specs=(vmem,) * 4,
        scratch_shapes=[pltpu.VMEM((rows, width), low)] * 5
        + [
            pltpu.VMEM(log_totals.shape, jnp.float32),
            pltpu.VMEM(block_picks.shape, jnp.int32),
            pltpu.VMEM((rows, local_width), low),
            dma((8,)),
        ]
        + [
            pltpu.VMEM((kvs, rows, 4 * hs), low),
            pltpu.VMEM((kvs, 8, rows), jnp.float32),
            pltpu.VMEM((kvs, rows, 4 * hs), low),
            pltpu.VMEM((kvs, 8, rows), jnp.float32),
            pltpu.VMEM((local_width, rows), low),
            pltpu.VMEM((tps, part, kvs * rows), low),
            pltpu.VMEM((hs, kvs * rows), jnp.float32),
            pltpu.VMEM((kvs, hs, kvs * rows), low),
            pltpu.VMEM((kvs, rows, 2 * hs), low),
            pltpu.VMEM((kvs, rows, 2 * hs), low),
        ]
        + [dma((kvs,))] * 6
        + [dma((tps,))] * 2
        + [dma((kvs,))] * 7,
        compiler_params=pltpu.CompilerParams(
            collective_id=0, has_side_effects=True, vmem_limit_bytes=67043328
        ),
    )(queries, keys, values, cotangent, attended, log_totals, block_picks, normed)


def device_part(*arrays):
    heads, kvs, tps = arrays[5].shape[0], lax.axis_size("kv"), lax.axis_size("tp")
    rows, width = arrays[0].shape
    if heads == kvs and kvs % (2 * tps) == 0 and rows == 2 * width // heads == 128 and kvs <= 8:
        return one_head(*arrays)
    if heads % kvs == 0:
        return by_heads(*arrays)
    return local(*arrays)


def solution(mesh):
    in_specs = (
        P("kv", "tp"),
        P("kv", "tp"),
        P("kv", "tp"),
        P("kv", "tp"),
        P("kv", "tp"),
        P("tp", "kv"),
        P("tp", "kv", None),
        P("kv", "tp"),
    )
    out_specs = (P("kv", "tp"), P("kv", "tp"), P("kv", "tp"), P("kv", "tp"))
    return jax.shard_map(device_part, mesh=mesh, in_specs=in_specs, out_specs=out_specs, check_vma=False)
```

profile of v0, /device:TPU:0, one launch (start us, length us, event | category | flops | bytes accessed | tf_op | source)
XLA Modules:
  0.0 58.7 jit_solution(7308767878342068166)
XLA Ops:
  0.6 52.5 %shard_map.111 = (bf16[128,512]{1,0:T(8,128)(2,1)}, bf16[128,512]{1,0:T(8,128)(2,1)}, bf16[128,512]{1,0:T(8,128)(2,1)}, f32[512,512]{1,0:T(8,128)}) custom-call(bf16[128,512]{1,0:T(8,128)(2,1)} %q_hbm.1, bf16[128,512]{1,0:T(8,128)(2,1)} %k_hbm.1, bf16[128,512]{1,0:T(8,128)(2,1)} %v_hbm.1, bf16[128,512]{1,0:T(8,128)(2,1)} %g_hbm.1, bf16[128,512]{1,0:T(8,128)(2,1)} %o_hbm.1, ...), custom_call_target="tpu_custom_call" | custom-call | tf_op jit(solution)/shard_map/pallas_call | solution.py:478
  53.2 0.0 copy-start.1
  53.2 1.6 %copy.16 = bf16[128,512]{1,0:T(8,128)(2,1)} copy(bf16[128,512]{1,0:T(8,128)(2,1)} %get-tuple-element.8) | data formatting | bytes 262144
  54.8 0.0 copy-done.1
  54.8 0.0 copy-start
  54.8 0.7 %copy.17 = bf16[128,512]{1,0:T(8,128)(2,1)} copy(bf16[128,512]{1,0:T(8,128)(2,1)S(1)} %copy-done.1) | data formatting | bytes 262144
  55.5 0.3 copy-done
  55.7 0.7 %copy.18 = bf16[128,512]{1,0:T(8,128)(2,1)} copy(bf16[128,512]{1,0:T(8,128)(2,1)S(1)} %copy-done) | data formatting | bytes 262144
  56.4 2.3 %copy.19 = f32[512,512]{1,0:T(8,128)} copy(f32[512,512]{1,0:T(8,128)} %get-tuple-element.11) | data formatting | bytes 2097152
Async XLA Ops:
  53.2 1.6 %copy-start.1 = (bf16[128,512]{1,0:T(8,128)(2,1)S(1)}, bf16[128,512]{1,0:T(8,128)(2,1)}, u32[]{:S(2)}) copy-start(bf16[128,512]{1,0:T(8,128)(2,1)} %get-tuple-element.9) | copy-start | bytes 393220
  54.8 1.0 %copy-start = (bf16[128,512]{1,0:T(8,128)(2,1)S(1)}, bf16[128,512]{1,0:T(8,128)(2,1)}, u32[]{:S(2)}) copy-start(bf16[128,512]{1,0:T(8,128)(2,1)} %get-tuple-element.10) | copy-start | bytes 393220
where the time goes:
time: 58.9 us; the launch traced here: 58.7 us
  Pallas kernels  52.5 us (89%)
  local copies, waits for them, and re-layouts  5.47 us (9%)
  between operations  0.65 us (1%)
    pallas_call x1, Pallas kernels, one_head(): pl.pallas_call(functools.partial(one_head_kernel, kvs, tps), out_shape=(j...  52.5 us
    unnamed x8, local copies, waits for them, and re-layouts  5.47 us

commit v1 on v0

--- a/solution.py
+++ b/solution.py
@@ -466,7 +466,31 @@
                 n1_copy(h, j).wait_send()
 
 
+def finish_kernel(count, *refs):
+    sources, places, done = refs[:count], refs[count : 2 * count], refs[2 * count]
+    copies = [
+        pltpu.make_async_copy(source, place, done.at[at])
+        for at, (source, place) in enumerate(zip(sources, places))
+    ]
+    for copy in copies[::-1]:
+        copy.start()
+    for copy in copies:
+        copy.wait()
+
+
+def finish(arrays):
+    count = len(arrays)
+    return pl.pallas_call(
+        functools.partial(finish_kernel, count),
+        out_shape=tuple(jax.ShapeDtypeStruct(a.shape, a.dtype) for a in arrays),
+        in_specs=[pl.BlockSpec(memory_space=pltpu.VMEM)] * count,
+        out_specs=(pl.BlockSpec(memory_space=pltpu.HBM),) * count,
+        scratch_shapes=[pltpu.SemaphoreType.DMA((count,))],
+    )(*[pltpu.with_memory_space_constraint(a, pltpu.VMEM) for a in arrays])
+
+
 def one_head(queries, keys, values, attended, cotangent, log_totals, block_picks, normed):
+    arrays = (queries, keys, values, cotangent, attended, log_totals, block_picks, normed)
     rows, width = queries.shape
     kvs, tps = lax.axis_size("kv"), lax.axis_size("tp")
     hs = width // kvs
@@ -475,13 +499,13 @@
     vmem = pl.BlockSpec(memory_space=pltpu.VMEM)
     dma = pltpu.SemaphoreType.DMA
     low = jnp.bfloat16
-    return pl.pallas_call(
+    outs = pl.pallas_call(
         functools.partial(one_head_kernel, kvs, tps),
         out_shape=(
-            jax.ShapeDtypeStruct((rows, width), low),
-            jax.ShapeDtypeStruct((rows, width), low),
-            jax.ShapeDtypeStruct((rows, width), low),
-            jax.ShapeDtypeStruct((tps * part, width), jnp.float32),
+            pltpu.VMEM((rows, width), low),
+            pltpu.VMEM((rows, width), low),
+            pltpu.VMEM((rows, width), low),
+            pltpu.VMEM((tps * part, width), jnp.float32),
         ),
         in_specs=[pl.BlockSpec(memory_space=pl.ANY)] * 8,
         out_specs=(vmem,) * 4,
@@ -508,9 +532,10 @@
         + [dma((tps,))] * 2
         + [dma((kvs,))] * 7,
         compiler_params=pltpu.CompilerParams(
-            collective_id=0, has_side_effects=True, vmem_limit_bytes=67043328
+            collective_id=0, has_side_effects=True, vmem_limit_bytes=40 * 2**20
         ),
-    )(queries, keys, values, cotangent, attended, log_totals, block_picks, normed)
+    )(*[pltpu.with_memory_space_constraint(a, pltpu.HBM) for a in arrays])
+    return finish(outs)
 
 
 def device_part(*arrays):

time: 58.9 us -> 53.3 us (0.905)
  local copies, waits for them, and re-layouts: 5.47 us -> 0 us
    unnamed x8 -> x0, local copies, waits for them, and re-layouts: 5.47 us -> none
    pallas_call x1 -> x2, Pallas kernels: 52.5 us -> 52.5 us  [the longest x1 51.4 us: one_head(): pl.pallas_call(functools.partial(one_head_kernel, kvs, tps), out_shape=(p...]
where the time goes in v1:
time: 53.3 us; the launch traced here: 53.2 us
  Pallas kernels  52.5 us (98%)
  between operations  0.64 us (1%)
    pallas_call x1, Pallas kernels, one_head(): pl.pallas_call(functools.partial(one_head_kernel, kvs, tps), out_shape=(p...  51.4 us
    pallas_call x1, Pallas kernels, finish(): pl.pallas_call(functools.partial(finish_kernel, count), out_shape=tuple((...  1.13 us

profile of v1, /device:TPU:0, one launch (start us, length us, event | category | flops | bytes accessed | tf_op | source)
XLA Modules:
  0.0 53.2 jit_solution(2039926262423919448)
XLA Ops:
  0.6 51.4 %shard_map.111 = (bf16[128,512]{1,0:T(8,128)(2,1)S(1)}, bf16[128,512]{1,0:T(8,128)(2,1)S(1)}, bf16[128,512]{1,0:T(8,128)(2,1)S(1)}, f32[512,512]{1,0:T(8,128)S(1)}) custom-call(bf16[128,512]{1,0:T(8,128)(2,1)} %q_hbm.1, bf16[128,512]{1,0:T(8,128)(2,1)} %k_hbm.1, bf16[128,512]{1,0:T(8,128)(2,1)} %v_hbm.1, bf16[128,512]{1,0:T(8,128)(2,1)} %g_hbm.1, ...), custom_call_target="tpu_custom_call" | custom-call | tf_op jit(solution)/shard_map/pallas_call | solution.py:502
  52.0 1.1 %shard_map.112 = (bf16[128,512]{1,0:T(8,128)(2,1)}, bf16[128,512]{1,0:T(8,128)(2,1)}, bf16[128,512]{1,0:T(8,128)(2,1)}, f32[512,512]{1,0:T(8,128)}) custom-call(bf16[128,512]{1,0:T(8,128)(2,1)S(1)} %get-tuple-element.8.refs_0_, bf16[128,512]{1,0:T(8,128)(2,1)S(1)} %get-tuple-element.9.refs_1_, bf16[128,512]{1,0:T(8,128)(2,1)S(1)} %get-tuple-element.10.refs_2_, ...), custom_call_target="tpu_custom_call" | custom-call | tf_op jit(solution)/shard_map/pallas_call | solution.py:483

commit v2 on v1

--- a/solution.py
+++ b/solution.py
@@ -190,8 +190,9 @@
     kvs, tps, q_hbm, k_hbm, v_hbm, g_hbm, o_hbm, log_hbm, picks_hbm, n_hbm,
     gq_ref, gk_ref, gv_ref, gw_ref,
     q_ref, k_ref, v_ref, g_ref, o_ref, log_ref, picks_ref, n_ref, load,
-    sent, sent_side, got, got_side, turned, feats, total, dq_all, dkv, dkv_got,
+    sent, sent_side, got, got_side, turned, plane, feats, total, dq_all, dkv, dkv_got,
     in_send, in_recv, side_send, side_recv, n1_send, n1_recv, n2_send, n2_recv,
+    y_send, y_recv, core_send, core_recv,
     up_send, down_send, mate_send, line_recv, mate_recv, dkv_send, dkv_recv,
 ):
     me, tp = lax.axis_index("kv"), lax.axis_index("tp")
@@ -199,7 +200,6 @@
     hs = width // kvs
     per = rows // BLOCK
     scale = hs ** (-0.5)
-    ratio = kvs // tps
     part = feats.shape[1]
 
     loads = []
@@ -210,19 +210,15 @@
         loads[-1].start()
 
     barrier = pltpu.get_barrier_semaphore()
-    count = kvs * tps
-
-    def greet(step, carry):
-        other = lax.rem(me * tps + tp + step, count)
+    deep = kvs // 2
+    spot, side_of = me // 2, lax.rem(me, 2)
+    mate = me + 1 - 2 * side_of
+    partners = [(lax.rem(me + d, kvs), tp) for d in range(1, kvs)]
+    partners += [(to, lax.rem(tp + d, tps)) for d in range(1, tps) for to in (me, mate)]
+    for partner in partners:
         pl.semaphore_signal(
-            barrier,
-            inc=1,
-            device_id=(other // tps, lax.rem(other, tps)),
-            device_id_type=pl.DeviceIdType.MESH,
+            barrier, inc=1, device_id=partner, device_id_type=pl.DeviceIdType.MESH
         )
-        return carry
-
-    lax.fori_loop(1, count, greet, 0)
     for copy in loads[:-1]:
         copy.wait()
 
@@ -250,7 +246,7 @@
     got[me] = sent[me]
     got_side[me] = sent_side[me]
 
-    pl.semaphore_wait(barrier, count - 1)
+    pl.semaphore_wait(barrier, len(partners))
 
     waits = []
     for d in range(1, kvs):
@@ -269,20 +265,25 @@
         turned[c, :] = n_ref[:, c].astype(jnp.float32).T.astype(jnp.bfloat16)
     here = pl.ds(pl.multiple_of(me * rows, rows), rows)
 
+    def side_rows(side):
+        return pl.ds(pl.multiple_of(side * rows, rows), rows)
+
+    def plane_rows(level):
+        return pl.ds(pl.multiple_of(level * 2 * rows, 2 * rows), 2 * rows)
+
     def n1_copy(h, j):
-        place = (h * tps + j) * part
         return remote(
-            turned.at[pl.ds(place, part)],
-            feats.at[j, :, here],
+            turned.at[pl.ds((h * tps + j) * part, part)],
+            plane.at[tp, :, side_rows(side_of)],
             n1_send.at[h * tps + j],
-            n1_recv.at[me],
-            ratio * tp + h,
+            n1_recv.at[side_of * tps + tp],
+            spot * 2 + h,
             j,
         )
 
-    for h in range(ratio):
+    for h in range(2):
         for j in range(tps):
-            mine = jnp.logical_and(me == ratio * tp + h, tp == j)
+            mine = jnp.logical_and(side_of == h, tp == j)
 
             @pl.when(jnp.logical_not(mine))
             def _():
@@ -291,7 +292,67 @@
             @pl.when(mine)
             def _():
                 place = (h * tps + j) * part
-                feats[j, :, here] = turned[place : place + part, :]
+                plane[j, :, h * rows : (h + 1) * rows] = turned[place : place + part, :]
+
+    for h in range(2):
+        for j in range(tps):
+
+            @pl.when(jnp.logical_not(jnp.logical_and(side_of == h, tp == j)))
+            def _():
+                remote(
+                    turned.at[pl.ds(0, part)],
+                    plane.at[j, :, side_rows(h)],
+                    n1_send.at[0],
+                    n1_recv.at[h * tps + j],
+                    me,
+                    tp,
+                ).wait_recv()
+
+    opposite, partner_core = lax.rem(tp + tps // 2, tps), tp + 1 - 2 * lax.rem(tp, 2)
+
+    def level_copy(d, level, at):
+        return remote(
+            plane.at[level],
+            feats.at[tp, :, plane_rows(at)],
+            n2_send.at[d],
+            n2_recv.at[d],
+            level * 2 + side_of,
+            tp,
+        )
+
+    for d in range(1, deep):
+        copy = level_copy(d, lax.rem(spot + d, deep), spot)
+        copy.start()
+        waits.append(copy)
+    feats[tp, :, plane_rows(spot)] = plane[spot]
+
+    def chunk_copy(d, owner, own, send, recv, at, to):
+        rows_of = feats.at[owner, :, plane_rows(lax.rem(spot + deep - d, deep))]
+        source = plane.at[spot] if own and d == 0 else rows_of
+        return remote(source, rows_of, send.at[at], recv.at[at], me, to)
+
+    def over_y(d, owner):
+        return chunk_copy(d, owner, True, y_send, y_recv, d, opposite)
+
+    def over_core(d, owner, relayed):
+        return chunk_copy(
+            d, owner, not relayed, core_send, core_recv, relayed * deep + d, partner_core
+        )
+
+    def pass_chunk(d):
+        if d:
+            level_copy(d, spot, lax.rem(spot + deep - d, deep)).wait_recv()
+        for copy in (over_y(d, tp), over_core(d, tp, 0)):
+            copy.start()
+            waits.append(copy)
+
+    def relay_chunk(d):
+        over_y(d, opposite).wait_recv()
+        copy = over_core(d, opposite, 1)
+        copy.start()
+        waits.append(copy)
+
+    pass_chunk(0)
 
     for d in range(1, kvs):
         src = lax.rem(me + kvs - d, kvs)
@@ -335,9 +396,6 @@
     dq_all[me] = (total[...] * scale).astype(jnp.bfloat16)
     dkv_got[me] = dkv[me]
 
-    deep = kvs // 2
-    spot, side_of = me // 2, lax.rem(me, 2)
-    mate = me + 1 - 2 * side_of
     half = hs // 2
     not_top, not_bottom = spot < deep - 1, spot > 0
 
@@ -373,24 +431,8 @@
         copy.start()
         waits.append(copy)
 
-    for k in range(kvs):
-
-        @pl.when(jnp.logical_not(jnp.logical_and(me == k, tp == me // ratio)))
-        def _():
-            remote(
-                turned.at[pl.ds(0, part)],
-                feats.at[tp, :, pl.ds(k * rows, rows)],
-                n1_send.at[0],
-                n1_recv.at[k],
-                me,
-                tp,
-            ).wait_recv()
-
-    for d in range(1, tps):
-        to = lax.rem(tp + d, tps)
-        copy = remote(feats.at[tp], feats.at[tp], n2_send.at[d], n2_recv.at[d], me, to)
-        copy.start()
-        waits.append(copy)
+    for d in range(1, deep):
+        pass_chunk(d)
 
     for z in range(1, deep):
         for piece in range(2):
@@ -414,6 +456,9 @@
                     downward(spot + z, piece).start()
 
                 across(spot + z, piece).start()
+
+        relay_chunk(z - 1)
+    relay_chunk(deep - 1)
 
     for d in range(1, kvs):
         src = lax.rem(me + kvs - d, kvs)
@@ -426,11 +471,9 @@
         gk_ref[:, c] = jnp.concatenate([left[:, :hs], right[:, :hs]], axis=1)
         gv_ref[:, c] = jnp.concatenate([left[:, hs:], right[:, hs:]], axis=1)
 
-    for d in range(1, tps):
-        src = lax.rem(tp + tps - d, tps)
-        remote(
-            feats.at[src], feats.at[src], n2_send.at[d], n2_recv.at[d], me, src
-        ).wait_recv()
+    for d in range(deep):
+        over_core(d, partner_core, 0).wait_recv()
+        over_core(d, lax.rem(partner_core + tps // 2, tps), 1).wait_recv()
     step = jnp.where(spot < deep // 2, 1, deep - 1)
     for z in range(deep):
         unit = lax.rem(spot + z * step, deep)
@@ -457,11 +500,10 @@
 
     for copy in waits:
         copy.wait_send()
-    for h in range(ratio):
+    for h in range(2):
         for j in range(tps):
-            mine = jnp.logical_and(me == ratio * tp + h, tp == j)
-
-            @pl.when(jnp.logical_not(mine))
+
+            @pl.when(jnp.logical_not(jnp.logical_and(side_of == h, tp == j)))
             def _():
                 n1_copy(h, j).wait_send()
 
@@ -522,6 +564,7 @@
             pltpu.VMEM((kvs, rows, 4 * hs), low),
             pltpu.VMEM((kvs, 8, rows), jnp.float32),
             pltpu.VMEM((local_width, rows), low),
+            pltpu.VMEM((kvs // 2, part, 2 * rows), low),
             pltpu.VMEM((tps, part, kvs * rows), low),
             pltpu.VMEM((hs, kvs * rows), jnp.float32),
             pltpu.VMEM((kvs, hs, kvs * rows), low),
@@ -529,8 +572,8 @@
             pltpu.VMEM((kvs, rows, 2 * hs), low),
         ]
         + [dma((kvs,))] * 6
-        + [dma((tps,))] * 2
-        + [dma((kvs,))] * 7,
+        + [dma((kvs // 2,))] * 4
+        + [dma((kvs,))] * 9,
         compiler_params=pltpu.CompilerParams(
             collective_id=0, has_side_effects=True, vmem_limit_bytes=40 * 2**20
         ),
@@ -541,7 +584,7 @@
 def device_part(*arrays):
     heads, kvs, tps = arrays[5].shape[0], lax.axis_size("kv"), lax.axis_size("tp")
     rows, width = arrays[0].shape
-    if heads == kvs and kvs % (2 * tps) == 0 and rows == 2 * width // heads == 128 and kvs <= 8:
+    if heads == kvs and kvs == 2 * tps and tps == 4 and rows == 2 * width // heads == 128 and kvs <= 8:
         return one_head(*arrays)
     if heads % kvs == 0:
         return by_heads(*arrays)

time: 53.3 us -> 46.1 us (0.86)
  Pallas kernels: 52.5 us -> 45.3 us
    pallas_call x1, Pallas kernels: 51.4 us -> 44.2 us  [one_head(): pl.pallas_call(functools.partial(one_head_kernel, kvs, tps), out_shape=(p...]
where the time goes in v2:
time: 46.1 us; the launch traced here: 45.9 us
  Pallas kernels  45.3 us (98%)
  between operations  0.64 us (1%)
    pallas_call x1, Pallas kernels, one_head(): pl.pallas_call(functools.partial(one_head_kernel, kvs, tps), out_shape=(p...  44.2 us
    pallas_call x1, Pallas kernels, finish(): pl.pallas_call(functools.partial(finish_kernel, count), out_shape=tuple((...  1.13 us

profile of v2, /device:TPU:0, one launch (start us, length us, event | category | flops | bytes accessed | tf_op | source)
XLA Modules:
  0.0 45.9 jit_solution(13462116362402983931)
XLA Ops:
  0.6 44.2 %shard_map.111 = (bf16[128,512]{1,0:T(8,128)(2,1)S(1)}, bf16[128,512]{1,0:T(8,128)(2,1)S(1)}, bf16[128,512]{1,0:T(8,128)(2,1)S(1)}, f32[512,512]{1,0:T(8,128)S(1)}) custom-call(bf16[128,512]{1,0:T(8,128)(2,1)} %q_hbm.1, bf16[128,512]{1,0:T(8,128)(2,1)} %k_hbm.1, bf16[128,512]{1,0:T(8,128)(2,1)} %v_hbm.1, bf16[128,512]{1,0:T(8,128)(2,1)} %g_hbm.1, ...), custom_call_target="tpu_custom_call" | custom-call | tf_op jit(solution)/shard_map/pallas_call | solution.py:544
  44.8 1.1 %shard_map.112 = (bf16[128,512]{1,0:T(8,128)(2,1)}, bf16[128,512]{1,0:T(8,128)(2,1)}, bf16[128,512]{1,0:T(8,128)(2,1)}, f32[512,512]{1,0:T(8,128)}) custom-call(bf16[128,512]{1,0:T(8,128)(2,1)S(1)} %get-tuple-element.8.refs_0_, bf16[128,512]{1,0:T(8,128)(2,1)S(1)} %get-tuple-element.9.refs_1_, bf16[128,512]{1,0:T(8,128)(2,1)S(1)} %get-tuple-element.10.refs_2_, ...), custom_call_target="tpu_custom_call" | custom-call | tf_op jit(solution)/shard_map/pallas_call | solution.py:525

commit v3 on v2

--- a/solution.py
+++ b/solution.py
@@ -193,7 +193,7 @@
     sent, sent_side, got, got_side, turned, plane, feats, total, dq_all, dkv, dkv_got,
     in_send, in_recv, side_send, side_recv, n1_send, n1_recv, n2_send, n2_recv,
     y_send, y_recv, core_send, core_recv,
-    up_send, down_send, mate_send, line_recv, mate_recv, dkv_send, dkv_recv,
+    up_send, down_send, mate_send, line_recv, mate_recv, dkv_send, dkv_recv, inside, around,
 ):
     me, tp = lax.axis_index("kv"), lax.axis_index("tp")
     rows, width = q_ref.shape
@@ -213,19 +213,59 @@
     deep = kvs // 2
     spot, side_of = me // 2, lax.rem(me, 2)
     mate = me + 1 - 2 * side_of
-    partners = [(lax.rem(me + d, kvs), tp) for d in range(1, kvs)]
-    partners += [(to, lax.rem(tp + d, tps)) for d in range(1, tps) for to in (me, mate)]
-    for partner in partners:
+    opposite, partner_core = lax.rem(tp + tps // 2, tps), tp + 1 - 2 * lax.rem(tp, 2)
+    outer = jnp.logical_or(spot == 0, spot == deep - 1)
+    pair, second, last = spot + 1 - 2 * lax.rem(spot, 2), lax.rem(spot + 2, deep), deep - 1 - spot
+
+    def signal(semaphore, to):
         pl.semaphore_signal(
-            barrier, inc=1, device_id=partner, device_id_type=pl.DeviceIdType.MESH
+            semaphore, inc=1, device_id=to, device_id_type=pl.DeviceIdType.MESH
         )
-    for copy in loads[:-1]:
+
+    def greet(semaphore):
+        for to in ((mate, tp), (pair * 2 + side_of, tp), (me, opposite), (me, partner_core)):
+            signal(semaphore, to)
+
+        @pl.when(jnp.logical_not(outer))
+        def _():
+            signal(semaphore, (last * 2 + side_of, tp))
+
+    touching = 5 - outer.astype(jnp.int32)
+    greet(barrier)
+    for copy in loads[:4]:
         copy.wait()
 
     for h in range(kvs):
         c = slice(h * hs, (h + 1) * hs)
         sent[h, :, : 2 * hs] = jnp.concatenate([q_ref[:, c], k_ref[:, c]], axis=1)
         sent[h, :, 2 * hs :] = jnp.concatenate([v_ref[:, c], g_ref[:, c]], axis=1)
+    pl.semaphore_wait(barrier, touching)
+
+    def main_copy(to, at):
+        return remote(sent.at[to], got.at[me], in_send.at[at], in_recv.at[me], to, tp)
+
+    def side_copy(to, at):
+        return remote(
+            sent_side.at[to], got_side.at[me], side_send.at[at], side_recv.at[me], to, tp
+        )
+
+    straight, crossed = side_of, 1 - side_of
+    targets = [mate]
+    targets += [level * 2 + s for level in (pair, second, last) for s in (straight, crossed)]
+    mains = [main_copy(to, at) for at, to in enumerate(targets)]
+    to_mate, to_pair, to_pair_mate, to_second, to_second_mate, to_last, to_last_mate = mains
+    waits = list(mains)
+
+    greet(inside)
+    to_pair.start()
+
+    @pl.when(jnp.logical_not(outer))
+    def _():
+        to_last.start()
+
+    to_mate.start()
+    for copy in loads[4:-1]:
+        copy.wait()
     product = g_ref[...].astype(jnp.float32) * o_ref[...].astype(jnp.float32)
     high = product.astype(jnp.bfloat16)
     low = (product - high.astype(jnp.float32)).astype(jnp.bfloat16)
@@ -245,19 +285,27 @@
         sent_side[h] = lines
     got[me] = sent[me]
     got_side[me] = sent_side[me]
-
-    pl.semaphore_wait(barrier, len(partners))
-
-    waits = []
-    for d in range(1, kvs):
-        to = lax.rem(me + d, kvs)
-        side = remote(
-            sent_side.at[to], got_side.at[me], side_send.at[d], side_recv.at[d], to, tp
-        )
-        main = remote(sent.at[to], got.at[me], in_send.at[d], in_recv.at[d], to, tp)
-        side.start()
-        main.start()
-        waits += [side, main]
+    pl.semaphore_wait(inside, touching)
+    signal(around, (mate, tp))
+    signal(around, (second * 2 + side_of, tp))
+    to_pair_mate.start()
+
+    @pl.when(jnp.logical_not(outer))
+    def _():
+        to_last_mate.start()
+
+    to_second.start()
+    pl.semaphore_wait(around, 2)
+
+    @pl.when(outer)
+    def _():
+        to_last.start()
+        to_last_mate.start()
+
+    to_second_mate.start()
+    for at, to in enumerate(targets):
+        waits.append(side_copy(to, at))
+        waits[-1].start()
 
     loads[-1].wait()
     for b in range(n_ref.shape[1] // 128):
@@ -308,58 +356,70 @@
                     tp,
                 ).wait_recv()
 
-    opposite, partner_core = lax.rem(tp + tps // 2, tps), tp + 1 - 2 * lax.rem(tp, 2)
-
-    def level_copy(d, level, at):
+    levels = (spot, pair, second, last)
+
+    def level_copy(k, at):
         return remote(
-            plane.at[level],
+            plane.at[levels[k]],
             feats.at[tp, :, plane_rows(at)],
-            n2_send.at[d],
-            n2_recv.at[d],
-            level * 2 + side_of,
+            n2_send.at[k],
+            n2_recv.at[k],
+            levels[k] * 2 + side_of,
             tp,
         )
 
-    for d in range(1, deep):
-        copy = level_copy(d, lax.rem(spot + d, deep), spot)
-        copy.start()
-        waits.append(copy)
+    def start_level(inner_k, outer_k):
+        if inner_k == outer_k:
+            level_copy(inner_k, spot).start()
+        else:
+
+            @pl.when(outer)
+            def _():
+                level_copy(outer_k, spot).start()
+
+            @pl.when(jnp.logical_not(outer))
+            def _():
+                level_copy(inner_k, spot).start()
+
+    start_level(3, 2)
+    start_level(1, 1)
+    start_level(2, 3)
+    waits += [level_copy(k, spot) for k in range(1, deep)]
     feats[tp, :, plane_rows(spot)] = plane[spot]
 
-    def chunk_copy(d, owner, own, send, recv, at, to):
-        rows_of = feats.at[owner, :, plane_rows(lax.rem(spot + deep - d, deep))]
-        source = plane.at[spot] if own and d == 0 else rows_of
+    def chunk_copy(k, owner, own, send, recv, at, to):
+        rows_of = feats.at[owner, :, plane_rows(levels[k])]
+        source = plane.at[spot] if own and k == 0 else rows_of
         return remote(source, rows_of, send.at[at], recv.at[at], me, to)
 
-    def over_y(d, owner):
-        return chunk_copy(d, owner, True, y_send, y_recv, d, opposite)
-
-    def over_core(d, owner, relayed):
+    def over_y(k, owner):
+        return chunk_copy(k, owner, True, y_send, y_recv, k, opposite)
+
+    def over_core(k, owner, relayed):
         return chunk_copy(
-            d, owner, not relayed, core_send, core_recv, relayed * deep + d, partner_core
+            k, owner, not relayed, core_send, core_recv, relayed * deep + k, partner_core
         )
 
-    def pass_chunk(d):
-        if d:
-            level_copy(d, spot, lax.rem(spot + deep - d, deep)).wait_recv()
-        for copy in (over_y(d, tp), over_core(d, tp, 0)):
+    def pass_chunk(k):
+        if k:
+            level_copy(k, levels[k]).wait_recv()
+        for copy in (over_y(k, tp), over_core(k, tp, 0)):
             copy.start()
-            waits.append(copy)
-
-    def relay_chunk(d):
-        over_y(d, opposite).wait_recv()
-        copy = over_core(d, opposite, 1)
-        copy.start()
-        waits.append(copy)
-
+
+    def relay_chunk(k):
+        over_y(k, opposite).wait_recv()
+        over_core(k, opposite, 1).start()
+
+    waits += [over_y(k, tp) for k in range(deep)] + [over_core(k, tp, 0) for k in range(deep)]
+    waits += [over_core(k, opposite, 1) for k in range(deep)]
     pass_chunk(0)
 
     for d in range(1, kvs):
         src = lax.rem(me + kvs - d, kvs)
         remote(
-            sent_side.at[src], got_side.at[src], side_send.at[d], side_recv.at[d], src, tp
+            sent_side.at[src], got_side.at[src], side_send.at[d], side_recv.at[src], src, tp
         ).wait_recv()
-        remote(sent.at[src], got.at[src], in_send.at[d], in_recv.at[d], src, tp).wait_recv()
+        remote(sent.at[src], got.at[src], in_send.at[d], in_recv.at[src], src, tp).wait_recv()
 
     s_at = lax.broadcasted_iota(jnp.int32, (rows, rows), 0)
     t_at = lax.broadcasted_iota(jnp.int32, (rows, rows), 1)
@@ -396,12 +456,13 @@
     dq_all[me] = (total[...] * scale).astype(jnp.bfloat16)
     dkv_got[me] = dkv[me]
 
-    half = hs // 2
+    pieces = 4
+    piece_rows = hs // pieces
     not_top, not_bottom = spot < deep - 1, spot > 0
 
     def unit_copy(unit, piece, send, recv, column, to):
-        rows_of = dq_all.at[unit * 2 + column, piece * half : (piece + 1) * half]
-        at = unit * 2 + piece
+        rows_of = dq_all.at[unit * 2 + column, piece * piece_rows : (piece + 1) * piece_rows]
+        at = unit * pieces + piece
         return remote(rows_of, rows_of, send.at[at], recv.at[at], to, tp)
 
     def upward(unit, piece):
@@ -413,7 +474,7 @@
     def across(unit, piece):
         return unit_copy(unit, piece, mate_send, mate_recv, side_of, mate)
 
-    for piece in range(2):
+    for piece in range(pieces):
 
         @pl.when(not_top)
         def _():
@@ -423,19 +484,34 @@
         def _():
             downward(spot, piece).start()
 
-    for piece in range(2):
+    for piece in range(pieces):
         across(spot, piece).start()
-    for d in range(1, kvs):
-        to = lax.rem(me + d, kvs)
-        copy = remote(dkv.at[to], dkv_got.at[me], dkv_send.at[d], dkv_recv.at[d], to, tp)
-        copy.start()
-        waits.append(copy)
-
-    for d in range(1, deep):
-        pass_chunk(d)
+
+    low_half = spot < deep // 2
+
+    def dkv_copy(to, at):
+        return remote(dkv.at[to], dkv_got.at[me], dkv_send.at[at], dkv_recv.at[me], to, tp)
+
+    def near(side):
+        return dkv_copy(pair * 2 + side, 2 + side)
+
+    def far(step, side):
+        level = jnp.where(low_half, deep // 2 + step, deep // 2 - 1 - step)
+        return dkv_copy(level * 2 + side, 4 + 2 * step + side)
+
+    dkv_copy(mate, 0).start()
+    waits.append(dkv_copy(mate, 0))
+
+    @pl.when(outer)
+    def _():
+        for side in range(2):
+            near(side).start()
+
+    for k in range(1, deep):
+        pass_chunk(k)
 
     for z in range(1, deep):
-        for piece in range(2):
+        for piece in range(pieces):
 
             @pl.when(spot >= z)
             def _():
@@ -457,19 +533,19 @@
 
                 across(spot + z, piece).start()
 
+        if z == 2:
+            for far_copy in [far(step, side) for step in range(deep // 2) for side in range(2)]:
+                far_copy.start()
+                waits.append(far_copy)
+
+            @pl.when(jnp.logical_not(outer))
+            def _():
+                for side in range(2):
+                    near(side).start()
+
+            waits += [near(side) for side in range(2)]
         relay_chunk(z - 1)
     relay_chunk(deep - 1)
-
-    for d in range(1, kvs):
-        src = lax.rem(me + kvs - d, kvs)
-        remote(
-            dkv.at[src], dkv_got.at[src], dkv_send.at[d], dkv_recv.at[d], src, tp
-        ).wait_recv()
-    for p in range(kvs // 2):
-        c = slice(p * 2 * hs, (p + 1) * 2 * hs)
-        left, right = dkv_got[2 * p], dkv_got[2 * p + 1]
-        gk_ref[:, c] = jnp.concatenate([left[:, :hs], right[:, :hs]], axis=1)
-        gv_ref[:, c] = jnp.concatenate([left[:, hs:], right[:, hs:]], axis=1)
 
     for d in range(deep):
         over_core(d, partner_core, 0).wait_recv()
@@ -477,7 +553,7 @@
     step = jnp.where(spot < deep // 2, 1, deep - 1)
     for z in range(deep):
         unit = lax.rem(spot + z * step, deep)
-        for piece in range(2):
+        for piece in range(pieces):
             unit_copy(unit, piece, mate_send, mate_recv, 1 - side_of, me).wait_recv()
         c = pl.ds(pl.multiple_of(unit * 2 * hs, 2 * hs), 2 * hs)
         pair = dq_all[pl.ds(unit * 2, 2), :, here].reshape(2 * hs, rows)
@@ -486,8 +562,19 @@
         for j in range(tps):
             gw_ref[j * part : (j + 1) * part, c] = mm(feats[j], cols, LAST)
 
+    for d in range(1, kvs):
+        src = lax.rem(me + kvs - d, kvs)
+        remote(
+            dkv.at[src], dkv_got.at[src], dkv_send.at[d], dkv_recv.at[src], src, tp
+        ).wait_recv()
+    for p in range(kvs // 2):
+        c = slice(p * 2 * hs, (p + 1) * 2 * hs)
+        left, right = dkv_got[2 * p], dkv_got[2 * p + 1]
+        gk_ref[:, c] = jnp.concatenate([left[:, :hs], right[:, :hs]], axis=1)
+        gv_ref[:, c] = jnp.concatenate([left[:, hs:], right[:, hs:]], axis=1)
+
     for unit in range(deep):
-        for piece in range(2):
+        for piece in range(pieces):
             across(unit, piece).wait_send()
 
             @pl.when(jnp.logical_and(not_top, unit <= spot))
@@ -573,7 +660,10 @@
         ]
         + [dma((kvs,))] * 6
         + [dma((kvs // 2,))] * 4
-        + [dma((kvs,))] * 9,
+        + [dma((kvs,))] * 2
+        + [dma((2 * kvs,))] * 5
+        + [dma((kvs,))] * 2
+        + [pltpu.SemaphoreType.REGULAR] * 2,
         compiler_params=pltpu.CompilerParams(
             collective_id=0, has_side_effects=True, vmem_limit_bytes=40 * 2**20
         ),

time: 46.1 us -> 44.1 us (0.957)
  Pallas kernels: 45.3 us -> 43.3 us
    pallas_call x1, Pallas kernels: 44.2 us -> 42.2 us  [one_head(): pl.pallas_call(functools.partial(one_head_kernel, kvs, tps), out_shape=(p...]
where the time goes in v3:
time: 44.1 us; the launch traced here: 44 us
  Pallas kernels  43.3 us (98%)
  between operations  0.64 us (1%)
    pallas_call x1, Pallas kernels, one_head(): pl.pallas_call(functools.partial(one_head_kernel, kvs, tps), out_shape=(p...  42.2 us
    pallas_call x1, Pallas kernels, finish(): pl.pallas_call(functools.partial(finish_kernel, count), out_shape=tuple((...  1.13 us

profile of v3, /device:TPU:0, one launch (start us, length us, event | category | flops | bytes accessed | tf_op | source)
XLA Modules:
  0.0 44.0 jit_solution(17655426706148102616)
XLA Ops:
  0.6 42.2 %shard_map.111 = (bf16[128,512]{1,0:T(8,128)(2,1)S(1)}, bf16[128,512]{1,0:T(8,128)(2,1)S(1)}, bf16[128,512]{1,0:T(8,128)(2,1)S(1)}, f32[512,512]{1,0:T(8,128)S(1)}) custom-call(bf16[128,512]{1,0:T(8,128)(2,1)} %q_hbm.1, bf16[128,512]{1,0:T(8,128)(2,1)} %k_hbm.1, bf16[128,512]{1,0:T(8,128)(2,1)} %v_hbm.1, bf16[128,512]{1,0:T(8,128)(2,1)} %g_hbm.1, ...), custom_call_target="tpu_custom_call" | custom-call | tf_op jit(solution)/shard_map/pallas_call | solution.py:631
  42.9 1.1 %shard_map.112 = (bf16[128,512]{1,0:T(8,128)(2,1)}, bf16[128,512]{1,0:T(8,128)(2,1)}, bf16[128,512]{1,0:T(8,128)(2,1)}, f32[512,512]{1,0:T(8,128)}) custom-call(bf16[128,512]{1,0:T(8,128)(2,1)S(1)} %get-tuple-element.8.refs_0_, bf16[128,512]{1,0:T(8,128)(2,1)S(1)} %get-tuple-element.9.refs_1_, bf16[128,512]{1,0:T(8,128)(2,1)S(1)} %get-tuple-element.10.refs_2_, ...), custom_call_target="tpu_custom_call" | custom-call | tf_op jit(solution)/shard_map/pallas_call | solution.py:612

commit v4 on v3

--- a/solution.py
+++ b/solution.py
@@ -263,7 +263,6 @@
     def _():
         to_last.start()
 
-    to_mate.start()
     for copy in loads[4:-1]:
         copy.wait()
     product = g_ref[...].astype(jnp.float32) * o_ref[...].astype(jnp.float32)
@@ -288,21 +287,23 @@
     pl.semaphore_wait(inside, touching)
     signal(around, (mate, tp))
     signal(around, (second * 2 + side_of, tp))
-    to_pair_mate.start()
+    to_second.start()
+    pl.semaphore_wait(around, 2)
+
+    @pl.when(outer)
+    def _():
+        to_last_mate.start()
+        to_last.start()
+
+    to_second_mate.start()
 
     @pl.when(jnp.logical_not(outer))
     def _():
         to_last_mate.start()
 
-    to_second.start()
-    pl.semaphore_wait(around, 2)
-
-    @pl.when(outer)
-    def _():
-        to_last.start()
-        to_last_mate.start()
-
-    to_second_mate.start()
+    to_pair_mate.start()
+    to_mate.start()
+
     for at, to in enumerate(targets):
         waits.append(side_copy(to, at))
         waits[-1].start()
@@ -427,6 +428,39 @@
     lines = [
         jnp.concatenate([got_side[m, r : r + 1] for m in range(kvs)], axis=1) for r in range(3)
     ]
+    pieces = 4
+    piece_columns = kvs * rows // pieces
+    not_top, not_bottom = spot < deep - 1, spot > 0
+
+    def unit_copy(unit, piece, send, recv, column, to):
+        columns = slice(piece * piece_columns, (piece + 1) * piece_columns)
+        columns_of = dq_all.at[unit * 2 + column, :, columns]
+        at = unit * pieces + piece
+        return remote(columns_of, columns_of, send.at[at], recv.at[at], to, tp)
+
+    def upward(unit, piece):
+        return unit_copy(unit, piece, up_send, line_recv, side_of, me + 2)
+
+    def downward(unit, piece):
+        return unit_copy(unit, piece, down_send, line_recv, side_of, me - 2)
+
+    def across(unit, piece):
+        return unit_copy(unit, piece, mate_send, mate_recv, side_of, mate)
+
+    def launch(piece):
+        columns = slice(piece * piece_columns, (piece + 1) * piece_columns)
+        dq_all[me, :, columns] = (total[:, columns] * scale).astype(jnp.bfloat16)
+
+        @pl.when(not_top)
+        def _():
+            upward(spot, piece).start()
+
+        @pl.when(not_bottom)
+        def _():
+            downward(spot, piece).start()
+
+        across(spot, piece).start()
+
     for i in range(kvs):
         late = (kvs - i) * rows
         q = got[i:, :, :hs].reshape(late, hs)
@@ -453,39 +487,15 @@
             total[...] = grad_q
         else:
             total[:, i * rows :] += grad_q
-    dq_all[me] = (total[...] * scale).astype(jnp.bfloat16)
+        if i == 1:
+            launch(0)
+        if i == 3:
+            launch(1)
+        if i == 5:
+            launch(2)
+        if i == 7:
+            launch(3)
     dkv_got[me] = dkv[me]
-
-    pieces = 4
-    piece_rows = hs // pieces
-    not_top, not_bottom = spot < deep - 1, spot > 0
-
-    def unit_copy(unit, piece, send, recv, column, to):
-        rows_of = dq_all.at[unit * 2 + column, piece * piece_rows : (piece + 1) * piece_rows]
-        at = unit * pieces + piece
-        return remote(rows_of, rows_of, send.at[at], recv.at[at], to, tp)
-
-    def upward(unit, piece):
-        return unit_copy(unit, piece, up_send, line_recv, side_of, me + 2)
-
-    def downward(unit, piece):
-        return unit_copy(unit, piece, down_send, line_recv, side_of, me - 2)
-
-    def across(unit, piece):
-        return unit_copy(unit, piece, mate_send, mate_recv, side_of, mate)
-
-    for piece in range(pieces):
-
-        @pl.when(not_top)
-        def _():
-            upward(spot, piece).start()
-
-        @pl.when(not_bottom)
-        def _():
-            downward(spot, piece).start()
-
-    for piece in range(pieces):
-        across(spot, piece).start()
 
     low_half = spot < deep // 2
 

time: 44.1 us -> 41.6 us (0.943)
  Pallas kernels: 43.3 us -> 40.8 us
    pallas_call x1, Pallas kernels: 42.2 us -> 39.7 us  [one_head(): pl.pallas_call(functools.partial(one_head_kernel, kvs, tps), out_shape=(p...]
where the time goes in v4:
time: 41.6 us; the launch traced here: 41.5 us
  Pallas kernels  40.8 us (98%)
  between operations  0.64 us (2%)
    pallas_call x1, Pallas kernels, one_head(): pl.pallas_call(functools.partial(one_head_kernel, kvs, tps), out_shape=(p...  39.7 us
    pallas_call x1, Pallas kernels, finish(): pl.pallas_call(functools.partial(finish_kernel, count), out_shape=tuple((...  1.13 us

profile of v4, /device:TPU:0, one launch (start us, length us, event | category | flops | bytes accessed | tf_op | source)
XLA Modules:
  0.0 41.5 jit_solution(17522266253378432520)
XLA Ops:
  0.6 39.7 %shard_map.111 = (bf16[128,512]{1,0:T(8,128)(2,1)S(1)}, bf16[128,512]{1,0:T(8,128)(2,1)S(1)}, bf16[128,512]{1,0:T(8,128)(2,1)S(1)}, f32[512,512]{1,0:T(8,128)S(1)}) custom-call(bf16[128,512]{1,0:T(8,128)(2,1)} %q_hbm.1, bf16[128,512]{1,0:T(8,128)(2,1)} %k_hbm.1, bf16[128,512]{1,0:T(8,128)(2,1)} %v_hbm.1, bf16[128,512]{1,0:T(8,128)(2,1)} %g_hbm.1, ...), custom_call_target="tpu_custom_call" | custom-call | tf_op jit(solution)/shard_map/pallas_call | solution.py:641
  40.4 1.1 %shard_map.112 = (bf16[128,512]{1,0:T(8,128)(2,1)}, bf16[128,512]{1,0:T(8,128)(2,1)}, bf16[128,512]{1,0:T(8,128)(2,1)}, f32[512,512]{1,0:T(8,128)}) custom-call(bf16[128,512]{1,0:T(8,128)(2,1)S(1)} %get-tuple-element.8.refs_0_, bf16[128,512]{1,0:T(8,128)(2,1)S(1)} %get-tuple-element.9.refs_1_, bf16[128,512]{1,0:T(8,128)(2,1)S(1)} %get-tuple-element.10.refs_2_, ...), custom_call_target="tpu_custom_call" | custom-call | tf_op jit(solution)/shard_map/pallas_call | solution.py:622

commit v5 on v4

--- a/solution.py
+++ b/solution.py
@@ -562,6 +562,18 @@
         over_core(d, lax.rem(partner_core + tps // 2, tps), 1).wait_recv()
     step = jnp.where(spot < deep // 2, 1, deep - 1)
     for z in range(deep):
+        if z == deep - 1:
+            for d in range(1, kvs):
+                src = lax.rem(me + kvs - d, kvs)
+                remote(
+                    dkv.at[src], dkv_got.at[src], dkv_send.at[d], dkv_recv.at[src], src, tp
+                ).wait_recv()
+            for p in range(kvs // 2):
+                c = slice(p * 2 * hs, (p + 1) * 2 * hs)
+                left, right = dkv_got[2 * p], dkv_got[2 * p + 1]
+                gk_ref[:, c] = jnp.concatenate([left[:, :hs], right[:, :hs]], axis=1)
+                gv_ref[:, c] = jnp.concatenate([left[:, hs:], right[:, hs:]], axis=1)
+
         unit = lax.rem(spot + z * step, deep)
         for piece in range(pieces):
             unit_copy(unit, piece, mate_send, mate_recv, 1 - side_of, me).wait_recv()
@@ -571,17 +583,6 @@
         cols = dq_all[pl.ds(unit * 2, 2)].reshape(2 * hs, kvs * rows)
         for j in range(tps):
             gw_ref[j * part : (j + 1) * part, c] = mm(feats[j], cols, LAST)
-
-    for d in range(1, kvs):
-        src = lax.rem(me + kvs - d, kvs)
-        remote(
-            dkv.at[src], dkv_got.at[src], dkv_send.at[d], dkv_recv.at[src], src, tp
-        ).wait_recv()
-    for p in range(kvs // 2):
-        c = slice(p * 2 * hs, (p + 1) * 2 * hs)
-        left, right = dkv_got[2 * p], dkv_got[2 * p + 1]
-        gk_ref[:, c] = jnp.concatenate([left[:, :hs], right[:, :hs]], axis=1)
-        gv_ref[:, c] = jnp.concatenate([left[:, hs:], right[:, hs:]], axis=1)
 
     for unit in range(deep):
         for piece in range(pieces):

time: 41.6 us -> 41.5 us (level)
  no operation moved by 1% of the time
where the time goes in v5:
time: 41.5 us; the launch traced here: 41.3 us
  Pallas kernels  40.7 us (98%)
  between operations  0.64 us (2%)
    pallas_call x1, Pallas kernels, one_head(): pl.pallas_call(functools.partial(one_head_kernel, kvs, tps), out_shape=(p...  39.6 us
    pallas_call x1, Pallas kernels, finish(): pl.pallas_call(functools.partial(finish_kernel, count), out_shape=tuple((...  1.13 us

profile of v5, /device:TPU:0, one launch (start us, length us, event | category | flops | bytes accessed | tf_op | source)
XLA Modules:
  0.0 41.3 jit_solution(15763047077484452831)
XLA Ops:
  0.6 39.6 %shard_map.111 = (bf16[128,512]{1,0:T(8,128)(2,1)S(1)}, bf16[128,512]{1,0:T(8,128)(2,1)S(1)}, bf16[128,512]{1,0:T(8,128)(2,1)S(1)}, f32[512,512]{1,0:T(8,128)S(1)}) custom-call(bf16[128,512]{1,0:T(8,128)(2,1)} %q_hbm.1, bf16[128,512]{1,0:T(8,128)(2,1)} %k_hbm.1, bf16[128,512]{1,0:T(8,128)(2,1)} %v_hbm.1, bf16[128,512]{1,0:T(8,128)(2,1)} %g_hbm.1, ...), custom_call_target="tpu_custom_call" | custom-call | tf_op jit(solution)/shard_map/pallas_call | solution.py:642
  40.2 1.1 %shard_map.112 = (bf16[128,512]{1,0:T(8,128)(2,1)}, bf16[128,512]{1,0:T(8,128)(2,1)}, bf16[128,512]{1,0:T(8,128)(2,1)}, f32[512,512]{1,0:T(8,128)}) custom-call(bf16[128,512]{1,0:T(8,128)(2,1)S(1)} %get-tuple-element.8.refs_0_, bf16[128,512]{1,0:T(8,128)(2,1)S(1)} %get-tuple-element.9.refs_1_, bf16[128,512]{1,0:T(8,128)(2,1)S(1)} %get-tuple-element.10.refs_2_, ...), custom_call_target="tpu_custom_call" | custom-call | tf_op jit(solution)/shard_map/pallas_call | solution.py:623
